TPU v7x, 32 devices: a whole 2x2x4 slice. The times are simulated.
32 devices in a mesh: row: 16 (over z, y, x), col: 2 (over core).
Axes of the slice: x: 2, y: 2, z: 4, core: 2. Of those that a mesh axis runs over, the one named last changes fastest.
Arguments:
- tokens: bfloat16 [2, 3072, 2048], P('col', 'row'), may hold values from -6 to 6
- proj_in: bfloat16 [2048, 512], P('col'), may hold values from -0.125 to 0.125
- proj_out: bfloat16 [512, 2048], P(None, 'row'), may hold values from -0.25 to 0.25
Outputs:
- output: bfloat16 [2, 3072, 2048], P('col', 'row')
All inputs are finite; a program needn't handle non-finite values.
Results may differ from a plain program's by a relative error of at most 0.0083.
Values may be sent and summed in bfloat16 or wider, within the bound.
No kernel may reach another device: no remote copies, remote signals or barrier semaphores. Data moves between devices by JAX's collectives and lax.ppermute only.
A program may use at most 64 MiB of HBM per device.

v0:
```python
import math

import jax
import jax.numpy as jnp
import numpy as np
from jax import lax
from jax.experimental import pallas as pl
from jax.experimental.pallas import tpu as pltpu
from jax.sharding import PartitionSpec as P


GRP = 128
LANES = 128
highest = lax.Precision.HIGHEST
span_inner = 128


def circle(height, breadth, period):
    product = lax.iota(jnp.int32, height)[:, None] * lax.iota(jnp.int32, breadth)[None, :] % period
    angle = product.astype(jnp.float32) * (2.0 * math.pi / period)
    return (jnp.cos(angle), jnp.sin(angle))


def positions(piece):
    real_in = piece[0, 0]
    imag_in = piece[1, 0]
    count, length = real_in.shape
    outer = length // span_inner
    real_in = real_in.reshape(count, outer, span_inner)
    imag_in = imag_in.reshape(count, outer, span_inner)
    cos_one, sin_one = circle(outer, outer, outer)
    first_re = jnp.einsum("ab,kbq->kaq", cos_one, real_in, precision=highest) - jnp.einsum(
        "ab,kbq->kaq", sin_one, imag_in, precision=highest
    )
    first_im = jnp.einsum("ab,kbq->kaq", sin_one, real_in, precision=highest) + jnp.einsum(
        "ab,kbq->kaq", cos_one, imag_in, precision=highest
    )
    twist_c, twist_s = circle(outer, span_inner, length)
    turned_re = first_re * twist_c - first_im * twist_s
    turned_im = first_re * twist_s + first_im * twist_c
    cos_two, sin_two = circle(span_inner, span_inner, span_inner)
    factor = 1.0 / math.sqrt(GRP * length)
    real_out = jnp.einsum("kaq,qb->kba", turned_re, cos_two, precision=highest) - jnp.einsum(
        "kaq,qb->kba", turned_im, sin_two, precision=highest
    )
    real_out = real_out.reshape(count, length) * factor
    return real_out[:, None, :]


def general_shards(tokens, proj_in, proj_out):
    seq_rows = tokens[0]
    local_len = seq_rows.shape[0]
    features = proj_in.shape[1]
    groups = features // GRP
    mapped = jnp.dot(
        seq_rows,
        lax.all_gather(proj_in, "col", axis=0, tiled=True),
        preferred_element_type=jnp.float32,
    ).astype(jnp.bfloat16)
    values = mapped.astype(jnp.float32).reshape(local_len, groups, GRP)
    cos_c, sin_c = circle(GRP, GRP, GRP)
    real_part = jnp.einsum("pgc,cs->gsp", values, cos_c, precision=highest)
    imag_part = jnp.einsum("pgc,cs->gsp", values, sin_c, precision=highest)
    ways = lax.axis_size("row")
    slots = groups * cos_c.shape[1]
    per_dev = slots // ways
    stacked = jnp.stack(
        [real_part.reshape(ways, per_dev, local_len), imag_part.reshape(ways, per_dev, local_len)],
        0,
    )
    spectra = positions(lax.all_to_all(stacked, "row", split_axis=1, concat_axis=3, tiled=True))
    outgoing = spectra.astype(jnp.bfloat16)
    back = lax.all_to_all(outgoing, "row", split_axis=2, concat_axis=0, tiled=True)
    mixed = back.reshape(features, local_len)
    result = lax.dot_general(
        mixed,
        lax.all_gather(proj_out, "row", axis=1, tiled=True),
        (((0,), (0,)), ((), ())),
        preferred_element_type=jnp.float32,
    )
    return result.astype(jnp.bfloat16)[None]


def channel_table(quarters, pairs):
    c = np.arange(GRP)
    rows = []
    for t in range(quarters):
        j = pairs * t + np.arange(pairs)
        angle = 2 * np.pi * (j[:, None] * c % GRP) / GRP
        sine = np.sin(angle)
        if t == 0:
            sine[0] = np.cos(np.pi * c)
        rows += [np.cos(angle), sine]
    return np.concatenate(rows, 0)


def channel_order(groups, quarters, pairs):
    order = []
    for g in range(groups):
        for t in range(quarters):
            j = pairs * t + np.arange(pairs)
            mirror = (GRP - j) % GRP
            if t == 0:
                mirror[0] = GRP // 2
            order += list(g * GRP + j) + list(g * GRP + mirror)
    return np.array(order)


def position_tables(ways, span):
    per = span // ways
    q = np.arange(span)
    low = min(LANES, span)
    even = np.zeros((ways, 16, 4 * LANES))
    odd = np.zeros((ways, 16, 4 * LANES))
    for owner in range(ways):
        for m in range(per):
            angle = 2 * np.pi * (q * (per * owner + m) % span) / span
            row = np.zeros(4 * LANES)
            row[:low] = np.cos(angle[:low])
            row[LANES : LANES + low] = np.sin(angle[:low])
            row[2 * LANES : 2 * LANES + span - low] = np.cos(angle[low:])
            row[3 * LANES : 3 * LANES + span - low] = np.sin(angle[low:])
            even[owner, m] = row
            odd[owner, m if m < 8 else m + 4] = row
    return even.reshape(-1, 4 * LANES), odd.reshape(-1, 4 * LANES)


def twiddle_table(ways, span):
    length = ways * span
    factor = 1.0 / math.sqrt(GRP * length)
    q = np.arange(2 * LANES)
    angle = 2 * np.pi * (np.arange(ways)[:, None] * q % length) / length
    cos, sin = np.cos(angle) * factor, np.sin(angle) * factor
    return np.stack([cos[:, :LANES], sin[:, :LANES], cos[:, LANES:], sin[:, LANES:]], 1)


def row_order(span):
    chunk = []
    chunk += [(0, m) for m in range(8)] + [(2, m) for m in range(8)]
    for a in range(4):
        chunk += [((0, 2, 1, 3)[a], 8 + m) for m in range(4)]
    chunk += [(1, m) for m in range(8)] + [(3, m) for m in range(8)]
    rows = len(chunk)
    hot = np.zeros((span, span))
    for b in range(4):
        for i, (a, m) in enumerate(chunk):
            hot[16 * m + 4 * a + b, b * rows + i] = 1
    return hot


def fetch_kernel(core, w_out, tok, w, table, mine, tok_copy, w_copy, table_copy, sems):
    half = mine.shape[0]
    rows = pl.ds(pl.multiple_of(core[0] * half, half), half)
    copies = [
        pltpu.make_async_copy(w_out.at[rows, :], mine, sems.at[0]),
        pltpu.make_async_copy(tok, tok_copy, sems.at[1]),
        pltpu.make_async_copy(w, w_copy, sems.at[2]),
        pltpu.make_async_copy(table, table_copy, sems.at[3]),
    ]
    for copy in copies:
        copy.start()
    for copy in copies:
        copy.wait()


def send_kernel(core, tok, w_own, w_other, table, out, padded):
    span, features = tok.shape[0], w_own.shape[1]
    depth = w_own.shape[0]
    columns = lambda which: pl.ds(pl.multiple_of(which * depth, depth), depth)
    mapped = jnp.dot(tok[:, columns(core[0])], w_own[...], preferred_element_type=jnp.float32) + jnp.dot(
        tok[:, columns(1 - core[0])], w_other[...], preferred_element_type=jnp.float32
    )
    padded[pl.ds(0, span), :] = mapped.astype(jnp.bfloat16)
    padded[pl.ds(span, 2 * LANES - span), :] = jnp.zeros((2 * LANES - span, features), jnp.bfloat16)
    groups = features // GRP
    quarters = out.shape[0] // groups
    for g in range(groups):
        turned = lax.dot_general(
            table[...],
            padded[:, g * GRP : (g + 1) * GRP],
            (((1,), (1,)), ((), ())),
            preferred_element_type=jnp.float32,
        )
        for t in range(quarters):
            cos = turned[32 * t : 32 * t + 16]
            sin = turned[32 * t + 16 : 32 * t + 32]
            high = cos[:, LANES:] + pltpu.roll(sin[:, LANES:], LANES // 2, 1)
            d = g * quarters + t
            out[d, 0:16, :] = cos[:, :LANES].astype(jnp.bfloat16)
            out[d, 16:32, :] = sin[:, :LANES].astype(jnp.bfloat16)
            out[d, 32:48, :] = high.astype(jnp.bfloat16)


def fft4(a, b, c, d):
    (ar, ai), (br, bi), (cr, ci), (dr, di) = a, b, c, d
    sr, si, tr, ti = ar + cr, ai + ci, ar - cr, ai - ci
    ur, ui, vr, vi = br + dr, bi + di, br - dr, bi - di
    return [(sr + ur, si + ui), (tr + vi, ti - vr), (sr - ur, si - ui), (tr - vi, ti + vr)]


def turn(v, n):
    re, im = v
    n %= 16
    if n == 0:
        return v
    if n == 4:
        return (im, -re)
    if n == 2:
        h = math.sqrt(0.5)
        return ((re + im) * h, (im - re) * h)
    if n == 6:
        h = math.sqrt(0.5)
        return ((im - re) * h, -(re + im) * h)
    c, s = math.cos(2 * math.pi * n / 16), math.sin(2 * math.pi * n / 16)
    return (re * c + im * s, im * c - re * s)


def fft16(v):
    inner = [fft4(v[a], v[a + 4], v[a + 8], v[a + 12]) for a in range(4)]
    out = [None] * 16
    for f in range(4):
        col = fft4(*[turn(inner[a][f], a * f) for a in range(4)])
        for e in range(4):
            out[f + 4 * e] = col[e]
    return out


def mix_kernel(special, x, even, odd, twist, out, turned):
    ways = x.shape[0]
    first = (lax.broadcasted_iota(jnp.int32, (16, LANES), 0) == 0) & (special[0] == 0)
    for part in range(2):
        v = []
        for r in range(ways):
            if part == 0:
                re = x[r, 0:16, :].astype(jnp.float32)
                im = -x[r, 16:32, :].astype(jnp.float32)
            else:
                re = x[r, 32:48, :].astype(jnp.float32)
                im = -pltpu.roll(re, LANES // 2, 1)
            v.append((re, im))
        spec = fft16(v)
        for k in range(ways):
            pr, pi = spec[k]
            qr, qi = spec[-k % ways]
            qi = -qi
            ur = jnp.where(first, (pr + qr) * 0.5, pr)
            ui = jnp.where(first, (pi + qi) * 0.5, pi)
            wr = jnp.where(first, (qi - pi) * 0.5, qr)
            wi = jnp.where(first, (pr - qr) * 0.5, qi)
            c = twist[k, 2 * part : 2 * part + 1, :]
            s = twist[k, 2 * part + 1 : 2 * part + 2, :]
            lo = slice(2 * part * LANES, (2 * part + 1) * LANES)
            hi = slice((2 * part + 1) * LANES, (2 * part + 2) * LANES)
            turned[32 * k : 32 * k + 16, lo] = (ur * c + ui * s).astype(jnp.bfloat16)
            turned[32 * k : 32 * k + 16, hi] = (ui * c - ur * s).astype(jnp.bfloat16)
            turned[32 * k + 16 : 32 * k + 32, lo] = (wr * c + wi * s).astype(jnp.bfloat16)
            turned[32 * k + 16 : 32 * k + 32, hi] = (wi * c - wr * s).astype(jnp.bfloat16)
    half = turned.shape[0] // 2
    nt = (((1,), (1,)), ((), ()))
    one = lax.dot_general(even[...], turned[:half, :], nt, preferred_element_type=jnp.float32)
    two = lax.dot_general(odd[...], turned[half:, :], nt, preferred_element_type=jnp.float32)
    for r in range(ways):
        e, o = one[16 * r : 16 * r + 16], two[16 * r : 16 * r + 16]
        tail = e[8:] + o[8:]
        left, right = slice(0, LANES), slice(LANES, 2 * LANES)
        out[r, 0:16, :] = jnp.concatenate([e[:8, left], o[:8, left]], 0).astype(jnp.bfloat16)
        out[r, 16:32, :] = jnp.concatenate([tail[:, left], tail[:, right]], 0).astype(jnp.bfloat16)
        out[r, 32:48, :] = jnp.concatenate([e[:8, right], o[:8, right]], 0).astype(jnp.bfloat16)


def gather_blocks(y, groups, stage):
    quarters = y.shape[0] // groups
    rows = y.shape[1]
    lane = lax.broadcasted_iota(jnp.int32, (rows, LANES), 1) // 32
    odd, high = lane % 2 == 1, lane >= 2
    for g in range(groups):
        v = [y[g * quarters + t].astype(jnp.float32) for t in range(quarters)]
        w = [None] * 4
        for t in (0, 2):
            w[t] = jnp.where(odd, pltpu.roll(v[t + 1], 32, 1), v[t])
            w[t + 1] = jnp.where(odd, v[t + 1], pltpu.roll(v[t], LANES - 32, 1))
        u = [None] * 4
        for b in (0, 1):
            u[b] = jnp.where(high, pltpu.roll(w[b + 2], 64, 1), w[b])
            u[b + 2] = jnp.where(high, w[b + 2], pltpu.roll(w[b], 64, 1))
        for b in range(4):
            stage[b * rows : (b + 1) * rows, g * GRP : (g + 1) * GRP] = u[b].astype(jnp.bfloat16)


def out_kernel(place, y, hot, swap, near, other, out, stage, mixed, held, sems):
    row, core = place[0], place[1]
    features = stage.shape[1]
    groups = features // GRP
    half = features // 2
    gather_blocks(y, groups, stage)
    rows = jnp.dot(hot[...], stage[...], preferred_element_type=jnp.float32).astype(jnp.bfloat16)
    for g in range(groups):
        part = slice(g * GRP, (g + 1) * GRP)
        mixed[:, part] = jnp.dot(rows[:, part], swap[...], preferred_element_type=jnp.float32).astype(jnp.bfloat16)
    left = mixed[:, pl.ds(pl.multiple_of(core * half, half), half)]
    right = mixed[:, pl.ds(pl.multiple_of((1 - core) * half, half), half)]
    ways = near.shape[0]
    copies = []
    for i in range(0, ways, 2):
        both = jnp.dot(
            left, jnp.concatenate([near[i], near[i + 1]], 1), preferred_element_type=jnp.float32
        ) + jnp.dot(right, jnp.concatenate([other[i], other[i + 1]], 1), preferred_element_type=jnp.float32)
        for n in range(2):
            plane, dz = (i + n) // (ways // 4), (i + n) % (ways // 4)
            owner = lax.bitwise_xor(lax.rem(row + 4 * dz, ways), plane)
            columns = pl.ds(pl.multiple_of(owner * LANES, LANES), LANES)
            held[:, columns] = both[:, n * LANES : (n + 1) * LANES].astype(jnp.bfloat16)
            copies.append(pltpu.make_async_copy(held.at[:, columns], out.at[:, columns], sems.at[i + n]))
            copies[-1].start()
    for copy in copies:
        copy.wait()


def vmem(count):
    return [pl.BlockSpec(memory_space=pltpu.VMEM)] * count


def shards(tokens, proj_in, proj_out):
    return fast_shards(tokens, proj_in, proj_out)


def fast_shards(tokens, proj_in, proj_out):
    seq_rows = tokens[0]
    span, _ = seq_rows.shape
    depth, features = proj_in.shape
    ways = lax.axis_size("row")
    groups = features // GRP
    quarters = ways // groups
    pairs = GRP // 2 // quarters
    bf16, f32 = jnp.bfloat16, jnp.float32
    room = pltpu.CompilerParams(vmem_limit_bytes=16 << 20)

    me = lax.axis_index("col")
    half = features // 2
    swap_cores = lambda v: lax.ppermute(v, "col", [(0, 1), (1, 0)])
    along = lambda v, to: lax.ppermute(v, ("row", "col"), [(2 * r + c, 2 * to(r, c) + c) for r in range(ways) for c in (0, 1)])
    other_w = swap_cores(proj_in)
    table = jnp.asarray(channel_table(quarters, pairs), bf16)
    hbm = pl.BlockSpec(memory_space=pltpu.MemorySpace.HBM)
    smem = pl.BlockSpec(memory_space=pltpu.SMEM)
    mine, tok, w_own, table = pl.pallas_call(
        fetch_kernel,
        in_specs=[smem] + [hbm] * 4,
        out_specs=vmem(4),
        out_shape=[
            jax.ShapeDtypeStruct((half, LANES), bf16),
            jax.ShapeDtypeStruct(seq_rows.shape, bf16),
            jax.ShapeDtypeStruct(proj_in.shape, bf16),
            jax.ShapeDtypeStruct(table.shape, bf16),
        ],
        scratch_shapes=[pltpu.SemaphoreType.DMA((4,))],
        compiler_params=room,
        name="fetch",
    )(me[None], *[pltpu.with_memory_space_constraint(v, pltpu.MemorySpace.HBM) for v in (proj_out, seq_rows, proj_in, table)])
    ring = [mine]
    for dz in range(1, ways // 4):
        ring.append(along(mine, lambda r, c: (r - 4 * dz) % ways))
    sent = pl.pallas_call(
        send_kernel,
        in_specs=[smem] + vmem(4),
        out_specs=vmem(1)[0],
        out_shape=jax.ShapeDtypeStruct((ways, 48, LANES), bf16),
        scratch_shapes=[pltpu.VMEM((2 * LANES, features), bf16)],
        cost_estimate=pl.CostEstimate(flops=2 * span * depth * features, bytes_accessed=2 << 20, transcendentals=0),
        compiler_params=room,
        name="send",
    )(me[None], tok, w_own, other_w, table)
    *ring, _ = lax.optimization_barrier((*ring, sent))
    ring = jnp.stack(ring, 0)
    planes = [along(ring, lambda r, c: r ^ flip) for flip in (1, 2, 3)]
    held = lax.all_to_all(sent, "row", 0, 0, tiled=True)

    even, odd = position_tables(ways, span)
    even, odd = jnp.asarray(even, bf16), jnp.asarray(odd, bf16)
    twist = jnp.asarray(twiddle_table(ways, span), f32)
    special = lax.rem(lax.axis_index("row"), quarters)[None]
    spectra = pl.pallas_call(
        mix_kernel,
        in_specs=[pl.BlockSpec(memory_space=pltpu.SMEM)] + vmem(4),
        out_specs=vmem(1)[0],
        out_shape=jax.ShapeDtypeStruct((ways, 48, LANES), bf16),
        scratch_shapes=[pltpu.VMEM((ways * 32, 4 * LANES), bf16)],
        compiler_params=room,
        name="mix",
    )(special, held, even, odd, twist)

    back = lax.all_to_all(spectra, "row", 0, 0, tiled=True)
    *planes, _ = lax.optimization_barrier((*planes, spectra))
    near = jnp.concatenate([ring] + planes, 0)
    other = swap_cores(near)
    hot = jnp.asarray(row_order(span), bf16)
    swap = np.zeros((GRP, GRP))
    swap[np.arange(GRP), channel_order(1, quarters, pairs)] = 1
    place = jnp.stack([lax.axis_index("row"), me])
    wide = ways * LANES
    result = pl.pallas_call(
        out_kernel,
        in_specs=[smem] + vmem(5),
        out_specs=hbm,
        out_shape=jax.ShapeDtypeStruct((span, wide), bf16),
        scratch_shapes=[
            pltpu.VMEM((span, features), bf16),
            pltpu.VMEM((span, features), bf16),
            pltpu.VMEM((span, wide), bf16),
            pltpu.SemaphoreType.DMA((ways,)),
        ],
        cost_estimate=pl.CostEstimate(flops=2 * span * wide * features, bytes_accessed=4 << 20, transcendentals=0),
        compiler_params=room,
        name="out",
    )(place, back, hot, jnp.asarray(swap, bf16), near, other)
    return result[None]


def fits(mesh, tokens, proj_in, proj_out):
    ways, cols = mesh.shape["row"], mesh.shape["col"]
    features = proj_in.shape[1]
    span = tokens.shape[1] // ways
    return (
        features % GRP == 0
        and ways == 4 * (features // GRP) == 16
        and span == 12 * ways
        and cols == 2
        and tokens.shape[0] == cols
        and proj_out.shape[1] == ways * LANES
    )


def solution(mesh):
    in_specs = (P("col", "row", None), P("col", None), P(None, "row"))
    out_specs = P("col", "row", None)

    def run(tokens, proj_in, proj_out):
        fast = fits(mesh, tokens, proj_in, proj_out)
        body = shards if fast else general_shards
        step = jax.shard_map(body, mesh=mesh, in_specs=in_specs, out_specs=out_specs, check_vma=False)
        return step(tokens, proj_in, proj_out)

    return run
```

profile of v0, /device:TPU:0, one launch (start us, length us, event | category | flops | bytes accessed | tf_op | source)
XLA Modules:
  0.0 49.0 jit_solution(5746367964704009028)
XLA Ops:
  0.0 0.5 %collective-permute-start = (bf16[1024,512]{1,0:T(8,128)(2,1)}, bf16[1024,512]{1,0:T(8,128)(2,1)S(1)}, u32[]{:S(2)}, u32[]{:S(2)}) collective-permute-start(bf16[1024,512]{1,0:T(8,128)(2,1)} %w.1), channel_id=1, source_target_pairs={{0,1},{1,0},{2,3},{3,2},{4,5},{5,4},{6,7},{7,6},{8,9},{9,8},{10,11... | collective-permute-start | bytes 3145736 | tf_op jit(solution)/shard_map/ppermute | solution.py:340
  0.5 1.5 %fetch.1 = (bf16[256,128]{1,0:T(8,128)(2,1)S(1)}, bf16[192,2048]{1,0:T(8,128)(2,1)S(1)}, bf16[1024,512]{1,0:T(8,128)(2,1)S(1)}, bf16[128,128]{1,0:T(8,128)(2,1)S(1)}) custom-call(s32[1]{0:T(128)} %bitcast.1.core, bf16[512,128]{1,0:T(8,128)(2,1)} %w_out.1, bf16[192,2048]{1,0:T(8,128)(2,1)} %bitcast.14, bf16[1024,512]{1,0:T(8,128)(2,1)} %w.1, ...), custom_call_target="tpu_custom_call" | custom-call | tf_op jit(solution)/shard_map/fetch/pallas_call | solution.py:346
  2.0 4.6 %collective-permute-start.1 = (bf16[256,128]{1,0:T(8,128)(2,1)S(1)}, bf16[256,128]{1,0:T(8,128)(2,1)S(1)}, u32[]{:S(2)}, u32[]{:S(2)}) collective-permute-start(bf16[256,128]{1,0:T(8,128)(2,1)S(1)} %get-tuple-element.20), channel_id=1, source_target_pairs={{0,24},{1,25},{2,26},{3,27},{4,28},{5,29},{6,30},{7,31},{8,0},{9,1... | collective-permute-start | bytes 196616 | tf_op jit(solution)/shard_map/ppermute | solution.py:341
  6.7 0.0 collective-permute-start.2
  6.7 1.0 %collective-permute-start.3 = (bf16[256,128]{1,0:T(8,128)(2,1)S(1)}, bf16[256,128]{1,0:T(8,128)(2,1)S(1)}, u32[]{:S(2)}, u32[]{:S(2)}) collective-permute-start(bf16[256,128]{1,0:T(8,128)(2,1)S(1)} %get-tuple-element.20), channel_id=1, source_target_pairs={{0,8},{1,9},{2,10},{3,11},{4,12},{5,13},{6,14},{7,15},{8,16},{9,17... | collective-permute-start | bytes 196616 | tf_op jit(solution)/shard_map/ppermute | solution.py:341
  7.7 0.0 collective-permute-done.w_other
  7.7 1.6 %send.1 = bf16[16,48,128]{2,1,0:T(8,128)(2,1)} custom-call(s32[1]{0:T(128)} %bitcast.1.core, bf16[192,2048]{1,0:T(8,128)(2,1)S(1)} %get-tuple-element.16.tok, bf16[1024,512]{1,0:T(8,128)(2,1)S(1)} %get-tuple-element.17.w_own, bf16[1024,512]{1,0:T(8,128)(2,1)S(1)} %collective-permute-done.w_other, bf16[128,128]{1,0:T(8,128)(2,1)S(1)} %get-tuple-element.18.table), custom_call_target="tpu_custom_call" | custom-call | flops 201326592 | bytes 2097152 | tf_op jit(solution)/shard_map/send/pallas_call | solution.py:363
  9.3 6.1 %all-to-all-start = ((bf16[16,48,128]{2,1,0:T(8,128)(2,1)}), bf16[16,48,128]{2,1,0:T(8,128)(2,1)S(1)}, u32[]{:S(2)}, u32[]{:S(2)}) async-start(bf16[16,48,128]{2,1,0:T(8,128)(2,1)} %send.1), calls=%async_computation | async-start | bytes 393216 | tf_op jit(solution)/shard_map/all_to_all | solution.py:376
  15.3 0.0 collective-permute-done.1
  15.4 0.0 collective-permute-done.2
  15.4 0.0 collective-permute-done.3
  15.4 0.0 copy-start.1
  15.4 0.0 copy-start
  15.5 2.0 %collective-permute-start.4 = (bf16[4,256,128]{2,1,0:T(8,128)(2,1)S(1)}, bf16[4,256,128]{2,1,0:T(8,128)(2,1)S(1)}, u32[]{:S(2)}, u32[]{:S(2)}) collective-permute-start(bf16[4,256,128]{2,1,0:T(8,128)(2,1)S(1)} %pad_maximum_fusion), channel_id=1, source_target_pairs={{0,2},{1,3},{2,0},{3,1},{4,6},{5,7},{6,4},{7,5},{8,10},{9,11},{10,... | collective-permute-start | bytes 786440 | tf_op jit(solution)/shard_map/ppermute | solution.py:341
  17.4 1.5 %collective-permute-start.5 = (bf16[4,256,128]{2,1,0:T(8,128)(2,1)S(1)}, bf16[4,256,128]{2,1,0:T(8,128)(2,1)S(1)}, u32[]{:S(2)}, u32[]{:S(2)}) collective-permute-start(bf16[4,256,128]{2,1,0:T(8,128)(2,1)S(1)} %pad_maximum_fusion), channel_id=1, source_target_pairs={{0,4},{1,5},{2,6},{3,7},{4,0},{5,1},{6,2},{7,3},{8,12},{9,13},{10,... | collective-permute-start | bytes 786440 | tf_op jit(solution)/shard_map/ppermute | solution.py:341
  18.9 0.1 collective-permute-start.6
  19.0 0.0 copy-start.4
  19.1 5.0 %all-to-all-done.x = bf16[16,48,128]{2,1,0:T(8,128)(2,1)S(1)} async-done(((bf16[16,48,128]{2,1,0:T(8,128)(2,1)}), bf16[16,48,128]{2,1,0:T(8,128)(2,1)S(1)}, u32[]{:S(2)}, u32[]{:S(2)}) %all-to-all-start) | async-done | bytes 196640 | tf_op jit(solution)/shard_map/all_to_all | solution.py:376
  24.1 0.0 copy-done.1
  24.1 1.3 %mix.1 = bf16[16,48,128]{2,1,0:T(8,128)(2,1)} custom-call(s32[1]{0:T(128)} %bitcast.2.special, bf16[16,48,128]{2,1,0:T(8,128)(2,1)S(1)} %all-to-all-done.x, bf16[256,512]{1,0:T(8,128)(2,1)S(1)} %copy-done, bf16[256,512]{1,0:T(8,128)(2,1)S(1)} %copy-done.1, f32[16,4,128]{2,1,0:T(4,128)S(1)} %copy-done.4), custom_call_target="tpu_custom_call" | custom-call | tf_op jit(solution)/shard_map/mix/pallas_call | solution.py:382
  25.4 1.3 %collective-permute-done.4 = bf16[4,256,128]{2,1,0:T(8,128)(2,1)S(1)} collective-permute-done((bf16[4,256,128]{2,1,0:T(8,128)(2,1)S(1)}, bf16[4,256,128]{2,1,0:T(8,128)(2,1)S(1)}, u32[]{:S(2)}, u32[]{:S(2)}) %collective-permute-start.4) | collective-permute-done | bytes 262176 | tf_op jit(solution)/shard_map/ppermute | solution.py:341
  26.7 4.1 %collective-permute-done.5 = bf16[4,256,128]{2,1,0:T(8,128)(2,1)S(1)} collective-permute-done((bf16[4,256,128]{2,1,0:T(8,128)(2,1)S(1)}, bf16[4,256,128]{2,1,0:T(8,128)(2,1)S(1)}, u32[]{:S(2)}, u32[]{:S(2)}) %collective-permute-start.5) | collective-permute-done | bytes 262176 | tf_op jit(solution)/shard_map/ppermute | solution.py:341
  30.8 1.2 %collective-permute-done.6 = bf16[4,256,128]{2,1,0:T(8,128)(2,1)S(1)} collective-permute-done((bf16[4,256,128]{2,1,0:T(8,128)(2,1)S(1)}, bf16[4,256,128]{2,1,0:T(8,128)(2,1)S(1)}, u32[]{:S(2)}, u32[]{:S(2)}) %collective-permute-start.6) | collective-permute-done | bytes 262176 | tf_op jit(solution)/shard_map/ppermute | solution.py:341
  32.1 0.0 copy-start.2
  32.1 0.0 copy-start.3
  32.1 0.1 collective-permute-start.7
  32.2 5.3 %all-to-all-start.1 = ((bf16[16,48,128]{2,1,0:T(8,128)(2,1)}), bf16[16,48,128]{2,1,0:T(8,128)(2,1)S(1)}, u32[]{:S(2)}, u32[]{:S(2)}) async-start(bf16[16,48,128]{2,1,0:T(8,128)(2,1)} %mix.1), calls=%async_computation.1 | async-start | bytes 393216 | tf_op jit(solution)/shard_map/all_to_all | solution.py:392
  37.5 0.1 pad_add_fusion.place
  37.6 8.9 %all-to-all-done.1.y = bf16[16,48,128]{2,1,0:T(8,128)(2,1)S(1)} async-done(((bf16[16,48,128]{2,1,0:T(8,128)(2,1)}), bf16[16,48,128]{2,1,0:T(8,128)(2,1)S(1)}, u32[]{:S(2)}, u32[]{:S(2)}) %all-to-all-start.1) | async-done | bytes 196640 | tf_op jit(solution)/shard_map/all_to_all | solution.py:392
  46.4 0.0 collective-permute-done.7.other
  46.4 0.0 copy-done.3
  46.4 2.5 %out.1 = bf16[192,2048]{1,0:T(8,128)(2,1)} custom-call(s32[2]{0:T(128)S(1)} %pad_add_fusion.place, bf16[16,48,128]{2,1,0:T(8,128)(2,1)S(1)} %all-to-all-done.1.y, bf16[192,192]{1,0:T(8,128)(2,1)S(1)} %copy-done.2, bf16[128,128]{1,0:T(8,128)(2,1)S(1)} %copy-done.3, bf16[16,256,128]{2,1,0:T(8,128)(2,1)S(1)} %constant_dynamic-update-slice_fusion.near, ...), custom_call_target="tpu_custom_call" | custom-call | flops 402653184 | bytes 4194304 | tf_op jit(solution)/shard_map/out/pallas_call | solution.py:401
  (11 shorter events, 0.2 us)
Async XLA Ops:
  0.0 7.7 %collective-permute-start = (bf16[1024,512]{1,0:T(8,128)(2,1)}, bf16[1024,512]{1,0:T(8,128)(2,1)S(1)}, u32[]{:S(2)}, u32[]{:S(2)}) collective-permute-start(bf16[1024,512]{1,0:T(8,128)(2,1)} %w.1), channel_id=1, source_target_pairs={{0,1},{1,0},{2,3},{3,2},{4,5},{5,4},{6,7},{7,6},{8,9},{9,8},{10,11... | collective-permute-start | bytes 3145736 | tf_op jit(solution)/shard_map/ppermute | solution.py:340
  2.0 13.3 %collective-permute-start.1 = (bf16[256,128]{1,0:T(8,128)(2,1)S(1)}, bf16[256,128]{1,0:T(8,128)(2,1)S(1)}, u32[]{:S(2)}, u32[]{:S(2)}) collective-permute-start(bf16[256,128]{1,0:T(8,128)(2,1)S(1)} %get-tuple-element.20), channel_id=1, source_target_pairs={{0,24},{1,25},{2,26},{3,27},{4,28},{5,29},{6,30},{7,31},{8,0},{9,1... | collective-permute-start | bytes 196616 | tf_op jit(solution)/shard_map/ppermute | solution.py:341
  6.7 8.7 %collective-permute-start.2 = (bf16[256,128]{1,0:T(8,128)(2,1)S(1)}, bf16[256,128]{1,0:T(8,128)(2,1)S(1)}, u32[]{:S(2)}, u32[]{:S(2)}) collective-permute-start(bf16[256,128]{1,0:T(8,128)(2,1)S(1)} %get-tuple-element.20), channel_id=1, source_target_pairs={{0,16},{1,17},{2,18},{3,19},{4,20},{5,21},{6,22},{7,23},{8,24},{9,... | collective-permute-start | bytes 196616 | tf_op jit(solution)/shard_map/ppermute | solution.py:341
  6.7 8.7 %collective-permute-start.3 = (bf16[256,128]{1,0:T(8,128)(2,1)S(1)}, bf16[256,128]{1,0:T(8,128)(2,1)S(1)}, u32[]{:S(2)}, u32[]{:S(2)}) collective-permute-start(bf16[256,128]{1,0:T(8,128)(2,1)S(1)} %get-tuple-element.20), channel_id=1, source_target_pairs={{0,8},{1,9},{2,10},{3,11},{4,12},{5,13},{6,14},{7,15},{8,16},{9,17... | collective-permute-start | bytes 196616 | tf_op jit(solution)/shard_map/ppermute | solution.py:341
  9.3 14.8 %all-to-all-start = ((bf16[16,48,128]{2,1,0:T(8,128)(2,1)}), bf16[16,48,128]{2,1,0:T(8,128)(2,1)S(1)}, u32[]{:S(2)}, u32[]{:S(2)}) async-start(bf16[16,48,128]{2,1,0:T(8,128)(2,1)} %send.1), calls=%async_computation | async-start | bytes 393216 | tf_op jit(solution)/shard_map/all_to_all | solution.py:376
  15.4 8.7 %copy-start.1 = (bf16[256,512]{1,0:T(8,128)(2,1)S(1)}, bf16[256,512]{1,0:T(8,128)(2,1)}, u32[]{:S(2)}) copy-start(bf16[256,512]{1,0:T(8,128)(2,1)} %constant.27.clone.odd) | copy-start | bytes 786436
  15.4 8.7 %copy-start = (bf16[256,512]{1,0:T(8,128)(2,1)S(1)}, bf16[256,512]{1,0:T(8,128)(2,1)}, u32[]{:S(2)}) copy-start(bf16[256,512]{1,0:T(8,128)(2,1)} %constant.26.clone.even) | copy-start | bytes 786436
  15.5 11.2 %collective-permute-start.4 = (bf16[4,256,128]{2,1,0:T(8,128)(2,1)S(1)}, bf16[4,256,128]{2,1,0:T(8,128)(2,1)S(1)}, u32[]{:S(2)}, u32[]{:S(2)}) collective-permute-start(bf16[4,256,128]{2,1,0:T(8,128)(2,1)S(1)} %pad_maximum_fusion), channel_id=1, source_target_pairs={{0,2},{1,3},{2,0},{3,1},{4,6},{5,7},{6,4},{7,5},{8,10},{9,11},{10,... | collective-permute-start | bytes 786440 | tf_op jit(solution)/shard_map/ppermute | solution.py:341
  17.4 13.3 %collective-permute-start.5 = (bf16[4,256,128]{2,1,0:T(8,128)(2,1)S(1)}, bf16[4,256,128]{2,1,0:T(8,128)(2,1)S(1)}, u32[]{:S(2)}, u32[]{:S(2)}) collective-permute-start(bf16[4,256,128]{2,1,0:T(8,128)(2,1)S(1)} %pad_maximum_fusion), channel_id=1, source_target_pairs={{0,4},{1,5},{2,6},{3,7},{4,0},{5,1},{6,2},{7,3},{8,12},{9,13},{10,... | collective-permute-start | bytes 786440 | tf_op jit(solution)/shard_map/ppermute | solution.py:341
  18.9 13.1 %collective-permute-start.6 = (bf16[4,256,128]{2,1,0:T(8,128)(2,1)S(1)}, bf16[4,256,128]{2,1,0:T(8,128)(2,1)S(1)}, u32[]{:S(2)}, u32[]{:S(2)}) collective-permute-start(bf16[4,256,128]{2,1,0:T(8,128)(2,1)S(1)} %pad_maximum_fusion), channel_id=1, source_target_pairs={{0,6},{1,7},{2,4},{3,5},{4,2},{5,3},{6,0},{7,1},{8,14},{9,15},{10,... | collective-permute-start | bytes 786440 | tf_op jit(solution)/shard_map/ppermute | solution.py:341
  19.0 5.1 %copy-start.4 = (f32[16,4,128]{2,1,0:T(4,128)S(1)}, f32[16,4,128]{2,1,0:T(4,128)}, u32[]{:S(2)}) copy-start(f32[16,4,128]{2,1,0:T(4,128)} %constant.28.clone.twist) | copy-start | bytes 98308
  32.1 14.3 %copy-start.2 = (bf16[192,192]{1,0:T(8,128)(2,1)S(1)}, bf16[192,192]{1,0:T(8,128)(2,1)}, u32[]{:S(2)}) copy-start(bf16[192,192]{1,0:T(8,128)(2,1)} %constant.29.clone.hot) | copy-start | bytes 221188
  32.1 14.3 %copy-start.3 = (bf16[128,128]{1,0:T(8,128)(2,1)S(1)}, bf16[128,128]{1,0:T(8,128)(2,1)}, u32[]{:S(2)}) copy-start(bf16[128,128]{1,0:T(8,128)(2,1)} %constant.30.clone.swap) | copy-start | bytes 98308
  32.1 14.3 %collective-permute-start.7 = (bf16[16,256,128]{2,1,0:T(8,128)(2,1)S(1)}, bf16[16,256,128]{2,1,0:T(8,128)(2,1)S(1)}, u32[]{:S(2)}, u32[]{:S(2)}) collective-permute-start(bf16[16,256,128]{2,1,0:T(8,128)(2,1)S(1)} %constant_dynamic-update-slice_fusion.near), channel_id=1, source_target_pairs={{0,1},{1,0},{2,3},{3,2},{4,5},{5,4},{6,7},{7,6},{8,9},{9,8},{10,11... | collective-permute-start | bytes 3145736 | tf_op jit(solution)/shard_map/ppermute | solution.py:340
  32.2 14.2 %all-to-all-start.1 = ((bf16[16,48,128]{2,1,0:T(8,128)(2,1)}), bf16[16,48,128]{2,1,0:T(8,128)(2,1)S(1)}, u32[]{:S(2)}, u32[]{:S(2)}) async-start(bf16[16,48,128]{2,1,0:T(8,128)(2,1)} %mix.1), calls=%async_computation.1 | async-start | bytes 393216 | tf_op jit(solution)/shard_map/all_to_all | solution.py:392
where the time goes:
time: 49.3 us; the launch traced here: 49 us
  starting transfers between devices  21.1 us (43%)
  waiting for transfers between devices  20.4 us (41%)
  Pallas kernels  6.93 us (14%)
    ppermute x6, starting transfers between devices, fast_shards(): lax.ppermute(v, ('row', 'col'), [(2 * r + c, 2 * to(r, c) + c) for r in r...  9.21 us
    all_to_all x1, waiting for transfers between devices, fast_shards(): back = lax.all_to_all(spectra, 'row', 0, 0, tiled=True)  8.87 us
    ppermute x6, waiting for transfers between devices, fast_shards(): lax.ppermute(v, ('row', 'col'), [(2 * r + c, 2 * to(r, c) + c) for r in r...  6.54 us
    all_to_all x1, starting transfers between devices, fast_shards(): held = lax.all_to_all(sent, 'row', 0, 0, tiled=True)  6.08 us
    all_to_all x1, starting transfers between devices, fast_shards(): back = lax.all_to_all(spectra, 'row', 0, 0, tiled=True)  5.28 us
    all_to_all x1, waiting for transfers between devices, fast_shards(): held = lax.all_to_all(sent, 'row', 0, 0, tiled=True)  5.02 us
    pallas_call x1, Pallas kernels, fast_shards(): pl.pallas_call(out_kernel, in_specs=[smem] + vmem(5), out_specs=hbm, out_...  2.53 us
    pallas_call x1, Pallas kernels, fast_shards(): pl.pallas_call(send_kernel, in_specs=[smem] + vmem(4), out_specs=vmem(1)[...  1.56 us
  transfers between devices with their start and end apart: 10, of which 5 were waited for; matrix products, arithmetic and copies ran while one was open for 0% of the time, Pallas kernels for 6%

commit v1 on v0

--- a/solution.py
+++ b/solution.py
@@ -148,18 +148,23 @@
     return hot
 
 
-def fetch_kernel(core, w_out, tok, w, table, mine, tok_copy, w_copy, table_copy, sems):
+def fetch_kernel(core, w_out, swap, w, table, mine, w_copy, table_copy, raw, hot, sems):
     half = mine.shape[0]
     rows = pl.ds(pl.multiple_of(core[0] * half, half), half)
     copies = [
-        pltpu.make_async_copy(w_out.at[rows, :], mine, sems.at[0]),
-        pltpu.make_async_copy(tok, tok_copy, sems.at[1]),
+        pltpu.make_async_copy(w_out.at[rows, :], raw, sems.at[0]),
+        pltpu.make_async_copy(swap, hot, sems.at[1]),
         pltpu.make_async_copy(w, w_copy, sems.at[2]),
         pltpu.make_async_copy(table, table_copy, sems.at[3]),
     ]
     for copy in copies:
         copy.start()
-    for copy in copies:
+    copies[0].wait()
+    copies[1].wait()
+    for g in range(half // GRP):
+        part = slice(g * GRP, (g + 1) * GRP)
+        mine[part, :] = jnp.dot(hot[...], raw[part, :], preferred_element_type=jnp.float32).astype(jnp.bfloat16)
+    for copy in copies[2:]:
         copy.wait()
 
 
@@ -287,26 +292,25 @@
             stage[b * rows : (b + 1) * rows, g * GRP : (g + 1) * GRP] = u[b].astype(jnp.bfloat16)
 
 
-def out_kernel(place, y, hot, swap, near, other, out, stage, mixed, held, sems):
+def out_kernel(place, y, hot, near, other, far, far_other, out, stage, mixed, held, sems):
     row, core = place[0], place[1]
     features = stage.shape[1]
     groups = features // GRP
     half = features // 2
     gather_blocks(y, groups, stage)
-    rows = jnp.dot(hot[...], stage[...], preferred_element_type=jnp.float32).astype(jnp.bfloat16)
-    for g in range(groups):
-        part = slice(g * GRP, (g + 1) * GRP)
-        mixed[:, part] = jnp.dot(rows[:, part], swap[...], preferred_element_type=jnp.float32).astype(jnp.bfloat16)
+    mixed[...] = jnp.dot(hot[...], stage[...], preferred_element_type=jnp.float32).astype(jnp.bfloat16)
     left = mixed[:, pl.ds(pl.multiple_of(core * half, half), half)]
     right = mixed[:, pl.ds(pl.multiple_of((1 - core) * half, half), half)]
-    ways = near.shape[0]
+    count = near.shape[0]
+    ways = count + far.shape[0]
     copies = []
     for i in range(0, ways, 2):
+        ours, theirs, at = (near, other, i) if i < count else (far, far_other, i - count)
         both = jnp.dot(
-            left, jnp.concatenate([near[i], near[i + 1]], 1), preferred_element_type=jnp.float32
-        ) + jnp.dot(right, jnp.concatenate([other[i], other[i + 1]], 1), preferred_element_type=jnp.float32)
+            left, jnp.concatenate([ours[at], ours[at + 1]], 1), preferred_element_type=jnp.float32
+        ) + jnp.dot(right, jnp.concatenate([theirs[at], theirs[at + 1]], 1), preferred_element_type=jnp.float32)
         for n in range(2):
-            plane, dz = (i + n) // (ways // 4), (i + n) % (ways // 4)
+            plane, dz = (1, 2, 0, 3)[(i + n) // (ways // 4)], (i + n) % (ways // 4)
             owner = lax.bitwise_xor(lax.rem(row + 4 * dz, ways), plane)
             columns = pl.ds(pl.multiple_of(owner * LANES, LANES), LANES)
             held[:, columns] = both[:, n * LANES : (n + 1) * LANES].astype(jnp.bfloat16)
@@ -341,22 +345,28 @@
     along = lambda v, to: lax.ppermute(v, ("row", "col"), [(2 * r + c, 2 * to(r, c) + c) for r in range(ways) for c in (0, 1)])
     other_w = swap_cores(proj_in)
     table = jnp.asarray(channel_table(quarters, pairs), bf16)
+    swap = np.zeros((GRP, GRP))
+    swap[np.arange(GRP), channel_order(1, quarters, pairs)] = 1
+    swap = jnp.asarray(swap, bf16)
     hbm = pl.BlockSpec(memory_space=pltpu.MemorySpace.HBM)
     smem = pl.BlockSpec(memory_space=pltpu.SMEM)
-    mine, tok, w_own, table = pl.pallas_call(
+    mine, w_own, table = pl.pallas_call(
         fetch_kernel,
         in_specs=[smem] + [hbm] * 4,
-        out_specs=vmem(4),
+        out_specs=vmem(3),
         out_shape=[
             jax.ShapeDtypeStruct((half, LANES), bf16),
-            jax.ShapeDtypeStruct(seq_rows.shape, bf16),
             jax.ShapeDtypeStruct(proj_in.shape, bf16),
             jax.ShapeDtypeStruct(table.shape, bf16),
         ],
-        scratch_shapes=[pltpu.SemaphoreType.DMA((4,))],
+        scratch_shapes=[
+            pltpu.VMEM((half, LANES), bf16),
+            pltpu.VMEM((GRP, GRP), bf16),
+            pltpu.SemaphoreType.DMA((4,)),
+        ],
         compiler_params=room,
         name="fetch",
-    )(me[None], *[pltpu.with_memory_space_constraint(v, pltpu.MemorySpace.HBM) for v in (proj_out, seq_rows, proj_in, table)])
+    )(me[None], *[pltpu.with_memory_space_constraint(v, pltpu.MemorySpace.HBM) for v in (proj_out, swap, proj_in, table)])
     ring = [mine]
     for dz in range(1, ways // 4):
         ring.append(along(mine, lambda r, c: (r - 4 * dz) % ways))
@@ -369,10 +379,12 @@
         cost_estimate=pl.CostEstimate(flops=2 * span * depth * features, bytes_accessed=2 << 20, transcendentals=0),
         compiler_params=room,
         name="send",
-    )(me[None], tok, w_own, other_w, table)
+    )(me[None], seq_rows, w_own, other_w, table)
     *ring, _ = lax.optimization_barrier((*ring, sent))
     ring = jnp.stack(ring, 0)
-    planes = [along(ring, lambda r, c: r ^ flip) for flip in (1, 2, 3)]
+    planes = []
+    for flip in (1, 2, 3):
+        planes.append(along(ring, lambda r, c: r ^ flip))
     held = lax.all_to_all(sent, "row", 0, 0, tiled=True)
 
     even, odd = position_tables(ways, span)
@@ -391,16 +403,16 @@
 
     back = lax.all_to_all(spectra, "row", 0, 0, tiled=True)
     *planes, _ = lax.optimization_barrier((*planes, spectra))
-    near = jnp.concatenate([ring] + planes, 0)
+    near = jnp.concatenate(planes[:2], 0)
+    far = jnp.concatenate([ring, planes[2]], 0)
     other = swap_cores(near)
+    far_other = swap_cores(far)
     hot = jnp.asarray(row_order(span), bf16)
-    swap = np.zeros((GRP, GRP))
-    swap[np.arange(GRP), channel_order(1, quarters, pairs)] = 1
     place = jnp.stack([lax.axis_index("row"), me])
     wide = ways * LANES
     result = pl.pallas_call(
         out_kernel,
-        in_specs=[smem] + vmem(5),
+        in_specs=[smem] + vmem(6),
         out_specs=hbm,
         out_shape=jax.ShapeDtypeStruct((span, wide), bf16),
         scratch_shapes=[
@@ -412,7 +424,7 @@
         cost_estimate=pl.CostEstimate(flops=2 * span * wide * features, bytes_accessed=4 << 20, transcendentals=0),
         compiler_params=room,
         name="out",
-    )(place, back, hot, jnp.asarray(swap, bf16), near, other)
+    )(place, back, hot, near, other, far, far_other)
     return result[None]
 
 

time: 49.3 us -> 47.9 us (0.972)
  starting transfers between devices: 21.1 us -> 20.5 us
    all_to_all x1, starting transfers between devices: 6.08 us -> 3.94 us  [fast_shards(): held = lax.all_to_all(sent, 'row', 0, 0, tiled=True)]
    ppermute x6, starting transfers between devices: 9.21 us -> 10.2 us  [fast_shards(): lax.ppermute(v, ('row', 'col'), [(2 * r + c, 2 * to(r, c) + c) for r in r...]
    ppermute x2 -> x3, starting transfers between devices: 0.56 us -> 1.12 us  [fast_shards(): swap_cores = lambda v: lax.ppermute(v, 'col', [(0, 1), (1, 0)])]
  transfers between devices with their start and end apart: 10 -> 11, of which waited for: 5 -> 5; matrix products, arithmetic and copies ran while one was open for 0% -> 0% of each run, Pallas kernels for 6% -> 6%
where the time goes in v1:
time: 47.9 us; the launch traced here: 47.5 us
  starting transfers between devices  20.5 us (43%)
  waiting for transfers between devices  20 us (42%)
  Pallas kernels  6.58 us (14%)
    ppermute x6, starting transfers between devices, fast_shards(): lax.ppermute(v, ('row', 'col'), [(2 * r + c, 2 * to(r, c) + c) for r in r...  10.2 us
    all_to_all x1, waiting for transfers between devices, fast_shards(): back = lax.all_to_all(spectra, 'row', 0, 0, tiled=True)  8.75 us
    ppermute x6, waiting for transfers between devices, fast_shards(): lax.ppermute(v, ('row', 'col'), [(2 * r + c, 2 * to(r, c) + c) for r in r...  6.39 us
    all_to_all x1, starting transfers between devices, fast_shards(): back = lax.all_to_all(spectra, 'row', 0, 0, tiled=True)  5.24 us
    all_to_all x1, waiting for transfers between devices, fast_shards(): held = lax.all_to_all(sent, 'row', 0, 0, tiled=True)  4.86 us
    all_to_all x1, starting transfers between devices, fast_shards(): held = lax.all_to_all(sent, 'row', 0, 0, tiled=True)  3.94 us
    pallas_call x1, Pallas kernels, fast_shards(): pl.pallas_call(out_kernel, in_specs=[smem] + vmem(6), out_specs=hbm, out_...  2.39 us
    pallas_call x1, Pallas kernels, fast_shards(): pl.pallas_call(send_kernel, in_specs=[smem] + vmem(4), out_specs=vmem(1)[...  1.56 us
  transfers between devices with their start and end apart: 11, of which 5 were waited for; matrix products, arithmetic and copies ran while one was open for 0% of the time, Pallas kernels for 6%

profile of v1, /device:TPU:0, one launch (start us, length us, event | category | flops | bytes accessed | tf_op | source)
XLA Modules:
  0.0 47.5 jit_solution(14793749764356015023)
XLA Ops:
  0.0 0.5 %collective-permute-start = (bf16[1024,512]{1,0:T(8,128)(2,1)}, bf16[1024,512]{1,0:T(8,128)(2,1)S(1)}, u32[]{:S(2)}, u32[]{:S(2)}) collective-permute-start(bf16[1024,512]{1,0:T(8,128)(2,1)} %w.1), channel_id=1, source_target_pairs={{0,1},{1,0},{2,3},{3,2},{4,5},{5,4},{6,7},{7,6},{8,9},{9,8},{10,11... | collective-permute-start | bytes 3145736 | tf_op jit(solution)/shard_map/ppermute | solution.py:344
  0.5 1.3 %fetch.1 = (bf16[256,128]{1,0:T(8,128)(2,1)S(1)}, bf16[1024,512]{1,0:T(8,128)(2,1)S(1)}, bf16[128,128]{1,0:T(8,128)(2,1)S(1)}) custom-call(s32[1]{0:T(128)} %bitcast.1.core, bf16[512,128]{1,0:T(8,128)(2,1)} %w_out.1, bf16[128,128]{1,0:T(8,128)(2,1)} %constant.26.clone.swap, bf16[1024,512]{1,0:T(8,128)(2,1)} %w.1, bf16[128,128]{1,0:T(8,128)(2,1)} %constant.25.clone.table), custom_call_target="tpu_custom_call" | custom-call | tf_op jit(solution)/shard_map/fetch/pallas_call | solution.py:353
  1.8 2.7 %collective-permute-start.3 = (bf16[256,128]{1,0:T(8,128)(2,1)S(1)}, bf16[256,128]{1,0:T(8,128)(2,1)S(1)}, u32[]{:S(2)}, u32[]{:S(2)}) collective-permute-start(bf16[256,128]{1,0:T(8,128)(2,1)S(1)} %get-tuple-element.18), channel_id=1, source_target_pairs={{0,8},{1,9},{2,10},{3,11},{4,12},{5,13},{6,14},{7,15},{8,16},{9,17... | collective-permute-start | bytes 196616 | tf_op jit(solution)/shard_map/ppermute | solution.py:345
  4.5 2.6 %collective-permute-start.2 = (bf16[256,128]{1,0:T(8,128)(2,1)S(1)}, bf16[256,128]{1,0:T(8,128)(2,1)S(1)}, u32[]{:S(2)}, u32[]{:S(2)}) collective-permute-start(bf16[256,128]{1,0:T(8,128)(2,1)S(1)} %get-tuple-element.18), channel_id=1, source_target_pairs={{0,16},{1,17},{2,18},{3,19},{4,20},{5,21},{6,22},{7,23},{8,24},{9,... | collective-permute-start | bytes 196616 | tf_op jit(solution)/shard_map/ppermute | solution.py:345
  7.1 1.3 %collective-permute-start.1 = (bf16[256,128]{1,0:T(8,128)(2,1)S(1)}, bf16[256,128]{1,0:T(8,128)(2,1)S(1)}, u32[]{:S(2)}, u32[]{:S(2)}) collective-permute-start(bf16[256,128]{1,0:T(8,128)(2,1)S(1)} %get-tuple-element.18), channel_id=1, source_target_pairs={{0,24},{1,25},{2,26},{3,27},{4,28},{5,29},{6,30},{7,31},{8,0},{9,1... | collective-permute-start | bytes 196616 | tf_op jit(solution)/shard_map/ppermute | solution.py:345
  8.5 0.0 collective-permute-done.w_other
  8.5 0.0 copy-done
  8.5 1.6 %send.1 = bf16[16,48,128]{2,1,0:T(8,128)(2,1)} custom-call(s32[1]{0:T(128)} %bitcast.1.core, bf16[192,2048]{1,0:T(8,128)(2,1)S(1)} %bitcast.13, bf16[1024,512]{1,0:T(8,128)(2,1)S(1)} %get-tuple-element.15.w_own, bf16[1024,512]{1,0:T(8,128)(2,1)S(1)} %collective-permute-done.w_other, bf16[128,128]{1,0:T(8,128)(2,1)S(1)} %get-tuple-element.16.table), custom_call_target="tpu_custom_call" | custom-call | flops 201326592 | bytes 2097152 | tf_op jit(solution)/shard_map/send/pallas_call | solution.py:373
  10.0 3.9 %all-to-all-start = ((bf16[16,48,128]{2,1,0:T(8,128)(2,1)}), bf16[16,48,128]{2,1,0:T(8,128)(2,1)S(1)}, u32[]{:S(2)}, u32[]{:S(2)}) async-start(bf16[16,48,128]{2,1,0:T(8,128)(2,1)} %send.1), calls=%async_computation | async-start | bytes 393216 | tf_op jit(solution)/shard_map/all_to_all | solution.py:388
  14.0 0.0 collective-permute-done.3
  14.0 0.0 collective-permute-done.2
  14.0 0.0 collective-permute-done.1
  14.0 0.0 copy-start.4
  14.1 0.0 copy-start.1
  14.1 0.0 copy-start.2
  14.1 2.9 %collective-permute-start.6 = (bf16[4,256,128]{2,1,0:T(8,128)(2,1)S(1)}, bf16[4,256,128]{2,1,0:T(8,128)(2,1)S(1)}, u32[]{:S(2)}, u32[]{:S(2)}) collective-permute-start(bf16[4,256,128]{2,1,0:T(8,128)(2,1)S(1)} %pad_maximum_fusion), channel_id=1, source_target_pairs={{0,6},{1,7},{2,4},{3,5},{4,2},{5,3},{6,0},{7,1},{8,14},{9,15},{10,... | collective-permute-start | bytes 786440 | tf_op jit(solution)/shard_map/ppermute | solution.py:345
  17.0 0.6 %collective-permute-start.5 = (bf16[4,256,128]{2,1,0:T(8,128)(2,1)S(1)}, bf16[4,256,128]{2,1,0:T(8,128)(2,1)S(1)}, u32[]{:S(2)}, u32[]{:S(2)}) collective-permute-start(bf16[4,256,128]{2,1,0:T(8,128)(2,1)S(1)} %pad_maximum_fusion), channel_id=1, source_target_pairs={{0,4},{1,5},{2,6},{3,7},{4,0},{5,1},{6,2},{7,3},{8,12},{9,13},{10,... | collective-permute-start | bytes 786440 | tf_op jit(solution)/shard_map/ppermute | solution.py:345
  17.5 0.1 collective-permute-start.4
  17.7 4.9 %all-to-all-done.x = bf16[16,48,128]{2,1,0:T(8,128)(2,1)S(1)} async-done(((bf16[16,48,128]{2,1,0:T(8,128)(2,1)}), bf16[16,48,128]{2,1,0:T(8,128)(2,1)S(1)}, u32[]{:S(2)}, u32[]{:S(2)}) %all-to-all-start) | async-done | bytes 196640 | tf_op jit(solution)/shard_map/all_to_all | solution.py:388
  22.6 1.3 %mix.1 = bf16[16,48,128]{2,1,0:T(8,128)(2,1)} custom-call(s32[1]{0:T(128)} %bitcast.2.special, bf16[16,48,128]{2,1,0:T(8,128)(2,1)S(1)} %all-to-all-done.x, bf16[256,512]{1,0:T(8,128)(2,1)S(1)} %copy-done.2, bf16[256,512]{1,0:T(8,128)(2,1)S(1)} %copy-done.1, f32[16,4,128]{2,1,0:T(4,128)S(1)} %copy-done.4), custom_call_target="tpu_custom_call" | custom-call | tf_op jit(solution)/shard_map/mix/pallas_call | solution.py:394
  23.9 2.1 %collective-permute-done.6 = bf16[4,256,128]{2,1,0:T(8,128)(2,1)S(1)} collective-permute-done((bf16[4,256,128]{2,1,0:T(8,128)(2,1)S(1)}, bf16[4,256,128]{2,1,0:T(8,128)(2,1)S(1)}, u32[]{:S(2)}, u32[]{:S(2)}) %collective-permute-start.6) | collective-permute-done | bytes 262176 | tf_op jit(solution)/shard_map/ppermute | solution.py:345
  26.0 4.1 %collective-permute-done.5 = bf16[4,256,128]{2,1,0:T(8,128)(2,1)S(1)} collective-permute-done((bf16[4,256,128]{2,1,0:T(8,128)(2,1)S(1)}, bf16[4,256,128]{2,1,0:T(8,128)(2,1)S(1)}, u32[]{:S(2)}, u32[]{:S(2)}) %collective-permute-start.5) | collective-permute-done | bytes 262176 | tf_op jit(solution)/shard_map/ppermute | solution.py:345
  30.1 0.2 collective-permute-done.4
  30.3 0.1 collective-permute-start.8
  30.4 0.0 copy-start.3
  30.5 0.6 %collective-permute-start.7 = (bf16[8,256,128]{2,1,0:T(8,128)(2,1)S(1)}, bf16[8,256,128]{2,1,0:T(8,128)(2,1)S(1)}, u32[]{:S(2)}, u32[]{:S(2)}) collective-permute-start(bf16[8,256,128]{2,1,0:T(8,128)(2,1)S(1)} %constant_dynamic-update-slice_fusion.near), channel_id=1, source_target_pairs={{0,1},{1,0},{2,3},{3,2},{4,5},{5,4},{6,7},{7,6},{8,9},{9,8},{10,11... | collective-permute-start | bytes 1572872 | tf_op jit(solution)/shard_map/ppermute | solution.py:344
  31.0 5.2 %all-to-all-start.1 = ((bf16[16,48,128]{2,1,0:T(8,128)(2,1)}), bf16[16,48,128]{2,1,0:T(8,128)(2,1)S(1)}, u32[]{:S(2)}, u32[]{:S(2)}) async-start(bf16[16,48,128]{2,1,0:T(8,128)(2,1)} %mix.1), calls=%async_computation.1 | async-start | bytes 393216 | tf_op jit(solution)/shard_map/all_to_all | solution.py:404
  36.3 0.1 pad_add_fusion.place
  36.3 8.8 %all-to-all-done.1.y = bf16[16,48,128]{2,1,0:T(8,128)(2,1)S(1)} async-done(((bf16[16,48,128]{2,1,0:T(8,128)(2,1)}), bf16[16,48,128]{2,1,0:T(8,128)(2,1)S(1)}, u32[]{:S(2)}, u32[]{:S(2)}) %all-to-all-start.1) | async-done | bytes 196640 | tf_op jit(solution)/shard_map/all_to_all | solution.py:404
  45.1 0.0 collective-permute-done.8.far_other
  45.1 0.0 collective-permute-done.7.other
  45.1 2.4 %out.1 = bf16[192,2048]{1,0:T(8,128)(2,1)} custom-call(s32[2]{0:T(128)S(1)} %pad_add_fusion.place, bf16[16,48,128]{2,1,0:T(8,128)(2,1)S(1)} %all-to-all-done.1.y, bf16[192,192]{1,0:T(8,128)(2,1)S(1)} %copy-done.3, bf16[8,256,128]{2,1,0:T(8,128)(2,1)S(1)} %constant_dynamic-update-slice_fusion.near, bf16[8,256,128]{2,1,0:T(8,128)(2,1)S(1)} %collective-permute-done.7.other, ...), custom_call_target="tpu_custom_call" | custom-call | flops 402653184 | bytes 4194304 | tf_op jit(solution)/shard_map/out/pallas_call | solution.py:413
  (13 shorter events, 0.2 us)
Async XLA Ops:
  0.0 8.5 %copy-start = (bf16[1,192,2048]{2,1,0:T(8,128)(2,1)S(1)}, bf16[1,192,2048]{2,1,0:T(8,128)(2,1)}, u32[]{:S(2)}) copy-start(bf16[1,192,2048]{2,1,0:T(8,128)(2,1)} %param.9) | copy-start | bytes 2359300
  0.0 8.5 %collective-permute-start = (bf16[1024,512]{1,0:T(8,128)(2,1)}, bf16[1024,512]{1,0:T(8,128)(2,1)S(1)}, u32[]{:S(2)}, u32[]{:S(2)}) collective-permute-start(bf16[1024,512]{1,0:T(8,128)(2,1)} %w.1), channel_id=1, source_target_pairs={{0,1},{1,0},{2,3},{3,2},{4,5},{5,4},{6,7},{7,6},{8,9},{9,8},{10,11... | collective-permute-start | bytes 3145736 | tf_op jit(solution)/shard_map/ppermute | solution.py:344
  1.8 12.1 %collective-permute-start.3 = (bf16[256,128]{1,0:T(8,128)(2,1)S(1)}, bf16[256,128]{1,0:T(8,128)(2,1)S(1)}, u32[]{:S(2)}, u32[]{:S(2)}) collective-permute-start(bf16[256,128]{1,0:T(8,128)(2,1)S(1)} %get-tuple-element.18), channel_id=1, source_target_pairs={{0,8},{1,9},{2,10},{3,11},{4,12},{5,13},{6,14},{7,15},{8,16},{9,17... | collective-permute-start | bytes 196616 | tf_op jit(solution)/shard_map/ppermute | solution.py:345
  4.5 9.5 %collective-permute-start.2 = (bf16[256,128]{1,0:T(8,128)(2,1)S(1)}, bf16[256,128]{1,0:T(8,128)(2,1)S(1)}, u32[]{:S(2)}, u32[]{:S(2)}) collective-permute-start(bf16[256,128]{1,0:T(8,128)(2,1)S(1)} %get-tuple-element.18), channel_id=1, source_target_pairs={{0,16},{1,17},{2,18},{3,19},{4,20},{5,21},{6,22},{7,23},{8,24},{9,... | collective-permute-start | bytes 196616 | tf_op jit(solution)/shard_map/ppermute | solution.py:345
  7.1 6.9 %collective-permute-start.1 = (bf16[256,128]{1,0:T(8,128)(2,1)S(1)}, bf16[256,128]{1,0:T(8,128)(2,1)S(1)}, u32[]{:S(2)}, u32[]{:S(2)}) collective-permute-start(bf16[256,128]{1,0:T(8,128)(2,1)S(1)} %get-tuple-element.18), channel_id=1, source_target_pairs={{0,24},{1,25},{2,26},{3,27},{4,28},{5,29},{6,30},{7,31},{8,0},{9,1... | collective-permute-start | bytes 196616 | tf_op jit(solution)/shard_map/ppermute | solution.py:345
  10.0 12.5 %all-to-all-start = ((bf16[16,48,128]{2,1,0:T(8,128)(2,1)}), bf16[16,48,128]{2,1,0:T(8,128)(2,1)S(1)}, u32[]{:S(2)}, u32[]{:S(2)}) async-start(bf16[16,48,128]{2,1,0:T(8,128)(2,1)} %send.1), calls=%async_computation | async-start | bytes 393216 | tf_op jit(solution)/shard_map/all_to_all | solution.py:388
  14.0 8.6 %copy-start.4 = (f32[16,4,128]{2,1,0:T(4,128)S(1)}, f32[16,4,128]{2,1,0:T(4,128)}, u32[]{:S(2)}) copy-start(f32[16,4,128]{2,1,0:T(4,128)} %constant.29.clone.twist) | copy-start | bytes 98308
  14.1 8.5 %copy-start.1 = (bf16[256,512]{1,0:T(8,128)(2,1)S(1)}, bf16[256,512]{1,0:T(8,128)(2,1)}, u32[]{:S(2)}) copy-start(bf16[256,512]{1,0:T(8,128)(2,1)} %constant.28.clone.odd) | copy-start | bytes 786436
  14.1 8.5 %copy-start.2 = (bf16[256,512]{1,0:T(8,128)(2,1)S(1)}, bf16[256,512]{1,0:T(8,128)(2,1)}, u32[]{:S(2)}) copy-start(bf16[256,512]{1,0:T(8,128)(2,1)} %constant.27.clone.even) | copy-start | bytes 786436
  14.1 11.9 %collective-permute-start.6 = (bf16[4,256,128]{2,1,0:T(8,128)(2,1)S(1)}, bf16[4,256,128]{2,1,0:T(8,128)(2,1)S(1)}, u32[]{:S(2)}, u32[]{:S(2)}) collective-permute-start(bf16[4,256,128]{2,1,0:T(8,128)(2,1)S(1)} %pad_maximum_fusion), channel_id=1, source_target_pairs={{0,6},{1,7},{2,4},{3,5},{4,2},{5,3},{6,0},{7,1},{8,14},{9,15},{10,... | collective-permute-start | bytes 786440 | tf_op jit(solution)/shard_map/ppermute | solution.py:345
  17.0 13.1 %collective-permute-start.5 = (bf16[4,256,128]{2,1,0:T(8,128)(2,1)S(1)}, bf16[4,256,128]{2,1,0:T(8,128)(2,1)S(1)}, u32[]{:S(2)}, u32[]{:S(2)}) collective-permute-start(bf16[4,256,128]{2,1,0:T(8,128)(2,1)S(1)} %pad_maximum_fusion), channel_id=1, source_target_pairs={{0,4},{1,5},{2,6},{3,7},{4,0},{5,1},{6,2},{7,3},{8,12},{9,13},{10,... | collective-permute-start | bytes 786440 | tf_op jit(solution)/shard_map/ppermute | solution.py:345
  17.5 12.7 %collective-permute-start.4 = (bf16[4,256,128]{2,1,0:T(8,128)(2,1)S(1)}, bf16[4,256,128]{2,1,0:T(8,128)(2,1)S(1)}, u32[]{:S(2)}, u32[]{:S(2)}) collective-permute-start(bf16[4,256,128]{2,1,0:T(8,128)(2,1)S(1)} %pad_maximum_fusion), channel_id=1, source_target_pairs={{0,2},{1,3},{2,0},{3,1},{4,6},{5,7},{6,4},{7,5},{8,10},{9,11},{10,... | collective-permute-start | bytes 786440 | tf_op jit(solution)/shard_map/ppermute | solution.py:345
  30.3 14.8 %collective-permute-start.8 = (bf16[8,256,128]{2,1,0:T(8,128)(2,1)S(1)}, bf16[8,256,128]{2,1,0:T(8,128)(2,1)S(1)}, u32[]{:S(2)}, u32[]{:S(2)}) collective-permute-start(bf16[8,256,128]{2,1,0:T(8,128)(2,1)S(1)} %constant_dynamic-update-slice_fusion.2.far), channel_id=1, source_target_pairs={{0,1},{1,0},{2,3},{3,2},{4,5},{5,4},{6,7},{7,6},{8,9},{9,8},{10,11... | collective-permute-start | bytes 1572872 | tf_op jit(solution)/shard_map/ppermute | solution.py:344
  30.4 14.7 %copy-start.3 = (bf16[192,192]{1,0:T(8,128)(2,1)S(1)}, bf16[192,192]{1,0:T(8,128)(2,1)}, u32[]{:S(2)}) copy-start(bf16[192,192]{1,0:T(8,128)(2,1)} %constant.30.clone.hot) | copy-start | bytes 221188
  30.5 14.6 %collective-permute-start.7 = (bf16[8,256,128]{2,1,0:T(8,128)(2,1)S(1)}, bf16[8,256,128]{2,1,0:T(8,128)(2,1)S(1)}, u32[]{:S(2)}, u32[]{:S(2)}) collective-permute-start(bf16[8,256,128]{2,1,0:T(8,128)(2,1)S(1)} %constant_dynamic-update-slice_fusion.near), channel_id=1, source_target_pairs={{0,1},{1,0},{2,3},{3,2},{4,5},{5,4},{6,7},{7,6},{8,9},{9,8},{10,11... | collective-permute-start | bytes 1572872 | tf_op jit(solution)/shard_map/ppermute | solution.py:344
  31.0 14.1 %all-to-all-start.1 = ((bf16[16,48,128]{2,1,0:T(8,128)(2,1)}), bf16[16,48,128]{2,1,0:T(8,128)(2,1)S(1)}, u32[]{:S(2)}, u32[]{:S(2)}) async-start(bf16[16,48,128]{2,1,0:T(8,128)(2,1)} %mix.1), calls=%async_computation.1 | async-start | bytes 393216 | tf_op jit(solution)/shard_map/all_to_all | solution.py:404

commit v2 on v1

--- a/solution.py
+++ b/solution.py
@@ -148,24 +148,20 @@
     return hot
 
 
-def fetch_kernel(core, w_out, swap, w, table, mine, w_copy, table_copy, raw, hot, sems):
+def fetch_kernel(core, w_out, swap, mine, raw, hot, sems):
     half = mine.shape[0]
     rows = pl.ds(pl.multiple_of(core[0] * half, half), half)
     copies = [
         pltpu.make_async_copy(w_out.at[rows, :], raw, sems.at[0]),
         pltpu.make_async_copy(swap, hot, sems.at[1]),
-        pltpu.make_async_copy(w, w_copy, sems.at[2]),
-        pltpu.make_async_copy(table, table_copy, sems.at[3]),
     ]
     for copy in copies:
         copy.start()
-    copies[0].wait()
-    copies[1].wait()
+    for copy in copies:
+        copy.wait()
     for g in range(half // GRP):
         part = slice(g * GRP, (g + 1) * GRP)
         mine[part, :] = jnp.dot(hot[...], raw[part, :], preferred_element_type=jnp.float32).astype(jnp.bfloat16)
-    for copy in copies[2:]:
-        copy.wait()
 
 
 def send_kernel(core, tok, w_own, w_other, table, out, padded):
@@ -304,12 +300,13 @@
     count = near.shape[0]
     ways = count + far.shape[0]
     copies = []
-    for i in range(0, ways, 2):
+    for i in range(0, ways, 4):
         ours, theirs, at = (near, other, i) if i < count else (far, far_other, i - count)
-        both = jnp.dot(
-            left, jnp.concatenate([ours[at], ours[at + 1]], 1), preferred_element_type=jnp.float32
-        ) + jnp.dot(right, jnp.concatenate([theirs[at], theirs[at + 1]], 1), preferred_element_type=jnp.float32)
-        for n in range(2):
+        wide = lambda blocks: jnp.concatenate([blocks[at + n] for n in range(4)], 1)
+        both = jnp.dot(left, wide(ours), preferred_element_type=jnp.float32) + jnp.dot(
+            right, wide(theirs), preferred_element_type=jnp.float32
+        )
+        for n in range(4):
             plane, dz = (1, 2, 0, 3)[(i + n) // (ways // 4)], (i + n) % (ways // 4)
             owner = lax.bitwise_xor(lax.rem(row + 4 * dz, ways), plane)
             columns = pl.ds(pl.multiple_of(owner * LANES, LANES), LANES)
@@ -350,23 +347,20 @@
     swap = jnp.asarray(swap, bf16)
     hbm = pl.BlockSpec(memory_space=pltpu.MemorySpace.HBM)
     smem = pl.BlockSpec(memory_space=pltpu.SMEM)
-    mine, w_own, table = pl.pallas_call(
+    mine = pl.pallas_call(
         fetch_kernel,
-        in_specs=[smem] + [hbm] * 4,
-        out_specs=vmem(3),
-        out_shape=[
-            jax.ShapeDtypeStruct((half, LANES), bf16),
-            jax.ShapeDtypeStruct(proj_in.shape, bf16),
-            jax.ShapeDtypeStruct(table.shape, bf16),
-        ],
+        in_specs=[smem] + [hbm] * 2,
+        out_specs=vmem(1)[0],
+        out_shape=jax.ShapeDtypeStruct((half, LANES), bf16),
         scratch_shapes=[
             pltpu.VMEM((half, LANES), bf16),
             pltpu.VMEM((GRP, GRP), bf16),
-            pltpu.SemaphoreType.DMA((4,)),
+            pltpu.SemaphoreType.DMA((2,)),
         ],
+        cost_estimate=pl.CostEstimate(flops=1 << 32, bytes_accessed=4 << 20, transcendentals=0),
         compiler_params=room,
         name="fetch",
-    )(me[None], *[pltpu.with_memory_space_constraint(v, pltpu.MemorySpace.HBM) for v in (proj_out, swap, proj_in, table)])
+    )(me[None], *[pltpu.with_memory_space_constraint(v, pltpu.MemorySpace.HBM) for v in (proj_out, swap)])
     ring = [mine]
     for dz in range(1, ways // 4):
         ring.append(along(mine, lambda r, c: (r - 4 * dz) % ways))
@@ -379,7 +373,7 @@
         cost_estimate=pl.CostEstimate(flops=2 * span * depth * features, bytes_accessed=2 << 20, transcendentals=0),
         compiler_params=room,
         name="send",
-    )(me[None], seq_rows, w_own, other_w, table)
+    )(me[None], seq_rows, proj_in, other_w, table)
     *ring, _ = lax.optimization_barrier((*ring, sent))
     ring = jnp.stack(ring, 0)
     planes = []

time: 47.9 us -> 47.7 us (level)
  transfers between devices with their start and end apart: 11 -> 11, of which waited for: 5 -> 5; matrix products, arithmetic and copies ran while one was open for 0% -> 0% of each run, Pallas kernels for 6% -> 5%
where the time goes in v2:
time: 47.7 us; the launch traced here: 47.3 us
  starting transfers between devices  20.4 us (43%)
  waiting for transfers between devices  20.1 us (42%)
  Pallas kernels  6.42 us (13%)
    ppermute x6, starting transfers between devices, fast_shards(): lax.ppermute(v, ('row', 'col'), [(2 * r + c, 2 * to(r, c) + c) for r in r...  10.1 us
    all_to_all x1, waiting for transfers between devices, fast_shards(): back = lax.all_to_all(spectra, 'row', 0, 0, tiled=True)  8.75 us
    ppermute x6, waiting for transfers between devices, fast_shards(): lax.ppermute(v, ('row', 'col'), [(2 * r + c, 2 * to(r, c) + c) for r in r...  6.4 us
    all_to_all x1, starting transfers between devices, fast_shards(): back = lax.all_to_all(spectra, 'row', 0, 0, tiled=True)  5.24 us
    all_to_all x1, waiting for transfers between devices, fast_shards(): held = lax.all_to_all(sent, 'row', 0, 0, tiled=True)  4.9 us
    all_to_all x1, starting transfers between devices, fast_shards(): held = lax.all_to_all(sent, 'row', 0, 0, tiled=True)  3.94 us
    pallas_call x1, Pallas kernels, fast_shards(): pl.pallas_call(out_kernel, in_specs=[smem] + vmem(6), out_specs=hbm, out_...  2.39 us
    pallas_call x1, Pallas kernels, fast_shards(): pl.pallas_call(send_kernel, in_specs=[smem] + vmem(4), out_specs=vmem(1)[...  1.57 us
  transfers between devices with their start and end apart: 11, of which 5 were waited for; matrix products, arithmetic and copies ran while one was open for 0% of the time, Pallas kernels for 5%

profile of v2, /device:TPU:0, one launch (start us, length us, event | category | flops | bytes accessed | tf_op | source)
XLA Modules:
  0.0 47.3 jit_solution(4436372534888238550)
XLA Ops:
  0.0 0.5 %collective-permute-start = (bf16[1024,512]{1,0:T(8,128)(2,1)}, bf16[1024,512]{1,0:T(8,128)(2,1)S(1)}, u32[]{:S(2)}, u32[]{:S(2)}) collective-permute-start(bf16[1024,512]{1,0:T(8,128)(2,1)} %w_own.1), channel_id=1, source_target_pairs={{0,1},{1,0},{2,3},{3,2},{4,5},{5,4},{6,7},{7,6},{8,9},{9,8},{10,11... | collective-permute-start | bytes 3145736 | tf_op jit(solution)/shard_map/ppermute | solution.py:341
  0.5 1.1 %fetch.1 = bf16[256,128]{1,0:T(8,128)(2,1)S(1)} custom-call(s32[1]{0:T(128)} %bitcast.1.core, bf16[512,128]{1,0:T(8,128)(2,1)} %w_out.1, bf16[128,128]{1,0:T(8,128)(2,1)} %constant.26.clone.swap), custom_call_target="tpu_custom_call" | custom-call | flops 4294967296 | bytes 4194304 | tf_op jit(solution)/shard_map/fetch/pallas_call | solution.py:350
  1.7 2.6 %collective-permute-start.3 = (bf16[256,128]{1,0:T(8,128)(2,1)S(1)}, bf16[256,128]{1,0:T(8,128)(2,1)S(1)}, u32[]{:S(2)}, u32[]{:S(2)}) collective-permute-start(bf16[256,128]{1,0:T(8,128)(2,1)S(1)} %fetch.1), channel_id=1, source_target_pairs={{0,8},{1,9},{2,10},{3,11},{4,12},{5,13},{6,14},{7,15},{8,16},{9,17... | collective-permute-start | bytes 196616 | tf_op jit(solution)/shard_map/ppermute | solution.py:342
  4.3 2.6 %collective-permute-start.2 = (bf16[256,128]{1,0:T(8,128)(2,1)S(1)}, bf16[256,128]{1,0:T(8,128)(2,1)S(1)}, u32[]{:S(2)}, u32[]{:S(2)}) collective-permute-start(bf16[256,128]{1,0:T(8,128)(2,1)S(1)} %fetch.1), channel_id=1, source_target_pairs={{0,16},{1,17},{2,18},{3,19},{4,20},{5,21},{6,22},{7,23},{8,24},{9,... | collective-permute-start | bytes 196616 | tf_op jit(solution)/shard_map/ppermute | solution.py:342
  6.9 1.3 %collective-permute-start.1 = (bf16[256,128]{1,0:T(8,128)(2,1)S(1)}, bf16[256,128]{1,0:T(8,128)(2,1)S(1)}, u32[]{:S(2)}, u32[]{:S(2)}) collective-permute-start(bf16[256,128]{1,0:T(8,128)(2,1)S(1)} %fetch.1), channel_id=1, source_target_pairs={{0,24},{1,25},{2,26},{3,27},{4,28},{5,29},{6,30},{7,31},{8,0},{9,1... | collective-permute-start | bytes 196616 | tf_op jit(solution)/shard_map/ppermute | solution.py:342
  8.2 0.0 collective-permute-done.w_other
  8.2 1.6 %send.1 = bf16[16,48,128]{2,1,0:T(8,128)(2,1)} custom-call(s32[1]{0:T(128)} %bitcast.1.core, bf16[192,2048]{1,0:T(8,128)(2,1)S(1)} %bitcast.13, bf16[1024,512]{1,0:T(8,128)(2,1)S(1)} %copy-done, bf16[1024,512]{1,0:T(8,128)(2,1)S(1)} %collective-permute-done.w_other, bf16[128,128]{1,0:T(8,128)(2,1)S(1)} %copy-done.5), custom_call_target="tpu_custom_call" | custom-call | flops 201326592 | bytes 2097152 | tf_op jit(solution)/shard_map/send/pallas_call | solution.py:367
  9.8 3.9 %all-to-all-start = ((bf16[16,48,128]{2,1,0:T(8,128)(2,1)}), bf16[16,48,128]{2,1,0:T(8,128)(2,1)S(1)}, u32[]{:S(2)}, u32[]{:S(2)}) async-start(bf16[16,48,128]{2,1,0:T(8,128)(2,1)} %send.1), calls=%async_computation | async-start | bytes 393216 | tf_op jit(solution)/shard_map/all_to_all | solution.py:382
  13.8 0.0 collective-permute-done.3
  13.8 0.0 collective-permute-done.2
  13.8 0.0 collective-permute-done.1
  13.8 0.0 copy-start.6
  13.8 0.0 copy-start.2
  13.9 0.0 copy-start.3
  13.9 2.9 %collective-permute-start.6 = (bf16[4,256,128]{2,1,0:T(8,128)(2,1)S(1)}, bf16[4,256,128]{2,1,0:T(8,128)(2,1)S(1)}, u32[]{:S(2)}, u32[]{:S(2)}) collective-permute-start(bf16[4,256,128]{2,1,0:T(8,128)(2,1)S(1)} %pad_maximum_fusion), channel_id=1, source_target_pairs={{0,6},{1,7},{2,4},{3,5},{4,2},{5,3},{6,0},{7,1},{8,14},{9,15},{10,... | collective-permute-start | bytes 786440 | tf_op jit(solution)/shard_map/ppermute | solution.py:342
  16.8 0.6 %collective-permute-start.5 = (bf16[4,256,128]{2,1,0:T(8,128)(2,1)S(1)}, bf16[4,256,128]{2,1,0:T(8,128)(2,1)S(1)}, u32[]{:S(2)}, u32[]{:S(2)}) collective-permute-start(bf16[4,256,128]{2,1,0:T(8,128)(2,1)S(1)} %pad_maximum_fusion), channel_id=1, source_target_pairs={{0,4},{1,5},{2,6},{3,7},{4,0},{5,1},{6,2},{7,3},{8,12},{9,13},{10,... | collective-permute-start | bytes 786440 | tf_op jit(solution)/shard_map/ppermute | solution.py:342
  17.3 0.1 collective-permute-start.4
  17.5 4.9 %all-to-all-done.x = bf16[16,48,128]{2,1,0:T(8,128)(2,1)S(1)} async-done(((bf16[16,48,128]{2,1,0:T(8,128)(2,1)}), bf16[16,48,128]{2,1,0:T(8,128)(2,1)S(1)}, u32[]{:S(2)}, u32[]{:S(2)}) %all-to-all-start) | async-done | bytes 196640 | tf_op jit(solution)/shard_map/all_to_all | solution.py:382
  22.4 0.0 copy-done.3
  22.4 1.3 %mix.1 = bf16[16,48,128]{2,1,0:T(8,128)(2,1)} custom-call(s32[1]{0:T(128)} %bitcast.2.special, bf16[16,48,128]{2,1,0:T(8,128)(2,1)S(1)} %all-to-all-done.x, bf16[256,512]{1,0:T(8,128)(2,1)S(1)} %copy-done.3, bf16[256,512]{1,0:T(8,128)(2,1)S(1)} %copy-done.2, f32[16,4,128]{2,1,0:T(4,128)S(1)} %copy-done.6), custom_call_target="tpu_custom_call" | custom-call | tf_op jit(solution)/shard_map/mix/pallas_call | solution.py:388
  23.7 2.1 %collective-permute-done.6 = bf16[4,256,128]{2,1,0:T(8,128)(2,1)S(1)} collective-permute-done((bf16[4,256,128]{2,1,0:T(8,128)(2,1)S(1)}, bf16[4,256,128]{2,1,0:T(8,128)(2,1)S(1)}, u32[]{:S(2)}, u32[]{:S(2)}) %collective-permute-start.6) | collective-permute-done | bytes 262176 | tf_op jit(solution)/shard_map/ppermute | solution.py:342
  25.8 4.2 %collective-permute-done.5 = bf16[4,256,128]{2,1,0:T(8,128)(2,1)S(1)} collective-permute-done((bf16[4,256,128]{2,1,0:T(8,128)(2,1)S(1)}, bf16[4,256,128]{2,1,0:T(8,128)(2,1)S(1)}, u32[]{:S(2)}, u32[]{:S(2)}) %collective-permute-start.5) | collective-permute-done | bytes 262176 | tf_op jit(solution)/shard_map/ppermute | solution.py:342
  29.9 0.2 collective-permute-done.4
  30.2 0.1 collective-permute-start.8
  30.3 0.0 copy-start.4
  30.3 0.6 %collective-permute-start.7 = (bf16[8,256,128]{2,1,0:T(8,128)(2,1)S(1)}, bf16[8,256,128]{2,1,0:T(8,128)(2,1)S(1)}, u32[]{:S(2)}, u32[]{:S(2)}) collective-permute-start(bf16[8,256,128]{2,1,0:T(8,128)(2,1)S(1)} %constant_dynamic-update-slice_fusion.near), channel_id=1, source_target_pairs={{0,1},{1,0},{2,3},{3,2},{4,5},{5,4},{6,7},{7,6},{8,9},{9,8},{10,11... | collective-permute-start | bytes 1572872 | tf_op jit(solution)/shard_map/ppermute | solution.py:341
  30.9 5.2 %all-to-all-start.1 = ((bf16[16,48,128]{2,1,0:T(8,128)(2,1)}), bf16[16,48,128]{2,1,0:T(8,128)(2,1)S(1)}, u32[]{:S(2)}, u32[]{:S(2)}) async-start(bf16[16,48,128]{2,1,0:T(8,128)(2,1)} %mix.1), calls=%async_computation.1 | async-start | bytes 393216 | tf_op jit(solution)/shard_map/all_to_all | solution.py:398
  36.1 0.1 pad_add_fusion.place
  36.2 8.8 %all-to-all-done.1.y = bf16[16,48,128]{2,1,0:T(8,128)(2,1)S(1)} async-done(((bf16[16,48,128]{2,1,0:T(8,128)(2,1)}), bf16[16,48,128]{2,1,0:T(8,128)(2,1)S(1)}, u32[]{:S(2)}, u32[]{:S(2)}) %all-to-all-start.1) | async-done | bytes 196640 | tf_op jit(solution)/shard_map/all_to_all | solution.py:398
  44.9 0.0 collective-permute-done.8.far_other
  44.9 0.0 collective-permute-done.7.other
  45.0 2.4 %out.1 = bf16[192,2048]{1,0:T(8,128)(2,1)} custom-call(s32[2]{0:T(128)S(1)} %pad_add_fusion.place, bf16[16,48,128]{2,1,0:T(8,128)(2,1)S(1)} %all-to-all-done.1.y, bf16[192,192]{1,0:T(8,128)(2,1)S(1)} %copy-done.4, bf16[8,256,128]{2,1,0:T(8,128)(2,1)S(1)} %constant_dynamic-update-slice_fusion.near, bf16[8,256,128]{2,1,0:T(8,128)(2,1)S(1)} %collective-permute-done.7.other, ...), custom_call_target="tpu_custom_call" | custom-call | flops 402653184 | bytes 4194304 | tf_op jit(solution)/shard_map/out/pallas_call | solution.py:407
  (17 shorter events, 0.2 us)
Async XLA Ops:
  0.0 8.2 %collective-permute-start = (bf16[1024,512]{1,0:T(8,128)(2,1)}, bf16[1024,512]{1,0:T(8,128)(2,1)S(1)}, u32[]{:S(2)}, u32[]{:S(2)}) collective-permute-start(bf16[1024,512]{1,0:T(8,128)(2,1)} %w_own.1), channel_id=1, source_target_pairs={{0,1},{1,0},{2,3},{3,2},{4,5},{5,4},{6,7},{7,6},{8,9},{9,8},{10,11... | collective-permute-start | bytes 3145736 | tf_op jit(solution)/shard_map/ppermute | solution.py:341
  0.5 7.7 %copy-start = (bf16[1024,512]{1,0:T(8,128)(2,1)S(1)}, bf16[1024,512]{1,0:T(8,128)(2,1)}, u32[]{:S(2)}) copy-start(bf16[1024,512]{1,0:T(8,128)(2,1)} %w_own.1) | copy-start | bytes 3145732
  0.5 7.7 %copy-start.1 = (bf16[1,192,2048]{2,1,0:T(8,128)(2,1)S(1)}, bf16[1,192,2048]{2,1,0:T(8,128)(2,1)}, u32[]{:S(2)}) copy-start(bf16[1,192,2048]{2,1,0:T(8,128)(2,1)} %param.9) | copy-start | bytes 2359300
  0.5 7.7 %copy-start.5 = (bf16[128,128]{1,0:T(8,128)(2,1)S(1)}, bf16[128,128]{1,0:T(8,128)(2,1)}, u32[]{:S(2)}) copy-start(bf16[128,128]{1,0:T(8,128)(2,1)} %constant.25.clone.table) | copy-start | bytes 98308
  1.7 12.1 %collective-permute-start.3 = (bf16[256,128]{1,0:T(8,128)(2,1)S(1)}, bf16[256,128]{1,0:T(8,128)(2,1)S(1)}, u32[]{:S(2)}, u32[]{:S(2)}) collective-permute-start(bf16[256,128]{1,0:T(8,128)(2,1)S(1)} %fetch.1), channel_id=1, source_target_pairs={{0,8},{1,9},{2,10},{3,11},{4,12},{5,13},{6,14},{7,15},{8,16},{9,17... | collective-permute-start | bytes 196616 | tf_op jit(solution)/shard_map/ppermute | solution.py:342
  4.3 9.5 %collective-permute-start.2 = (bf16[256,128]{1,0:T(8,128)(2,1)S(1)}, bf16[256,128]{1,0:T(8,128)(2,1)S(1)}, u32[]{:S(2)}, u32[]{:S(2)}) collective-permute-start(bf16[256,128]{1,0:T(8,128)(2,1)S(1)} %fetch.1), channel_id=1, source_target_pairs={{0,16},{1,17},{2,18},{3,19},{4,20},{5,21},{6,22},{7,23},{8,24},{9,... | collective-permute-start | bytes 196616 | tf_op jit(solution)/shard_map/ppermute | solution.py:342
  6.9 6.9 %collective-permute-start.1 = (bf16[256,128]{1,0:T(8,128)(2,1)S(1)}, bf16[256,128]{1,0:T(8,128)(2,1)S(1)}, u32[]{:S(2)}, u32[]{:S(2)}) collective-permute-start(bf16[256,128]{1,0:T(8,128)(2,1)S(1)} %fetch.1), channel_id=1, source_target_pairs={{0,24},{1,25},{2,26},{3,27},{4,28},{5,29},{6,30},{7,31},{8,0},{9,1... | collective-permute-start | bytes 196616 | tf_op jit(solution)/shard_map/ppermute | solution.py:342
  9.8 12.6 %all-to-all-start = ((bf16[16,48,128]{2,1,0:T(8,128)(2,1)}), bf16[16,48,128]{2,1,0:T(8,128)(2,1)S(1)}, u32[]{:S(2)}, u32[]{:S(2)}) async-start(bf16[16,48,128]{2,1,0:T(8,128)(2,1)} %send.1), calls=%async_computation | async-start | bytes 393216 | tf_op jit(solution)/shard_map/all_to_all | solution.py:382
  13.8 8.6 %copy-start.6 = (f32[16,4,128]{2,1,0:T(4,128)S(1)}, f32[16,4,128]{2,1,0:T(4,128)}, u32[]{:S(2)}) copy-start(f32[16,4,128]{2,1,0:T(4,128)} %constant.29.clone.twist) | copy-start | bytes 98308
  13.8 8.5 %copy-start.2 = (bf16[256,512]{1,0:T(8,128)(2,1)S(1)}, bf16[256,512]{1,0:T(8,128)(2,1)}, u32[]{:S(2)}) copy-start(bf16[256,512]{1,0:T(8,128)(2,1)} %constant.28.clone.odd) | copy-start | bytes 786436
  13.9 8.5 %copy-start.3 = (bf16[256,512]{1,0:T(8,128)(2,1)S(1)}, bf16[256,512]{1,0:T(8,128)(2,1)}, u32[]{:S(2)}) copy-start(bf16[256,512]{1,0:T(8,128)(2,1)} %constant.27.clone.even) | copy-start | bytes 786436
  13.9 11.9 %collective-permute-start.6 = (bf16[4,256,128]{2,1,0:T(8,128)(2,1)S(1)}, bf16[4,256,128]{2,1,0:T(8,128)(2,1)S(1)}, u32[]{:S(2)}, u32[]{:S(2)}) collective-permute-start(bf16[4,256,128]{2,1,0:T(8,128)(2,1)S(1)} %pad_maximum_fusion), channel_id=1, source_target_pairs={{0,6},{1,7},{2,4},{3,5},{4,2},{5,3},{6,0},{7,1},{8,14},{9,15},{10,... | collective-permute-start | bytes 786440 | tf_op jit(solution)/shard_map/ppermute | solution.py:342
  16.8 13.2 %collective-permute-start.5 = (bf16[4,256,128]{2,1,0:T(8,128)(2,1)S(1)}, bf16[4,256,128]{2,1,0:T(8,128)(2,1)S(1)}, u32[]{:S(2)}, u32[]{:S(2)}) collective-permute-start(bf16[4,256,128]{2,1,0:T(8,128)(2,1)S(1)} %pad_maximum_fusion), channel_id=1, source_target_pairs={{0,4},{1,5},{2,6},{3,7},{4,0},{5,1},{6,2},{7,3},{8,12},{9,13},{10,... | collective-permute-start | bytes 786440 | tf_op jit(solution)/shard_map/ppermute | solution.py:342
  17.3 12.8 %collective-permute-start.4 = (bf16[4,256,128]{2,1,0:T(8,128)(2,1)S(1)}, bf16[4,256,128]{2,1,0:T(8,128)(2,1)S(1)}, u32[]{:S(2)}, u32[]{:S(2)}) collective-permute-start(bf16[4,256,128]{2,1,0:T(8,128)(2,1)S(1)} %pad_maximum_fusion), channel_id=1, source_target_pairs={{0,2},{1,3},{2,0},{3,1},{4,6},{5,7},{6,4},{7,5},{8,10},{9,11},{10,... | collective-permute-start | bytes 786440 | tf_op jit(solution)/shard_map/ppermute | solution.py:342
  30.2 14.8 %collective-permute-start.8 = (bf16[8,256,128]{2,1,0:T(8,128)(2,1)S(1)}, bf16[8,256,128]{2,1,0:T(8,128)(2,1)S(1)}, u32[]{:S(2)}, u32[]{:S(2)}) collective-permute-start(bf16[8,256,128]{2,1,0:T(8,128)(2,1)S(1)} %constant_dynamic-update-slice_fusion.2.far), channel_id=1, source_target_pairs={{0,1},{1,0},{2,3},{3,2},{4,5},{5,4},{6,7},{7,6},{8,9},{9,8},{10,11... | collective-permute-start | bytes 1572872 | tf_op jit(solution)/shard_map/ppermute | solution.py:341
  30.3 14.7 %copy-start.4 = (bf16[192,192]{1,0:T(8,128)(2,1)S(1)}, bf16[192,192]{1,0:T(8,128)(2,1)}, u32[]{:S(2)}) copy-start(bf16[192,192]{1,0:T(8,128)(2,1)} %constant.30.clone.hot) | copy-start | bytes 221188
  30.3 14.6 %collective-permute-start.7 = (bf16[8,256,128]{2,1,0:T(8,128)(2,1)S(1)}, bf16[8,256,128]{2,1,0:T(8,128)(2,1)S(1)}, u32[]{:S(2)}, u32[]{:S(2)}) collective-permute-start(bf16[8,256,128]{2,1,0:T(8,128)(2,1)S(1)} %constant_dynamic-update-slice_fusion.near), channel_id=1, source_target_pairs={{0,1},{1,0},{2,3},{3,2},{4,5},{5,4},{6,7},{7,6},{8,9},{9,8},{10,11... | collective-permute-start | bytes 1572872 | tf_op jit(solution)/shard_map/ppermute | solution.py:341
  30.9 14.1 %all-to-all-start.1 = ((bf16[16,48,128]{2,1,0:T(8,128)(2,1)}), bf16[16,48,128]{2,1,0:T(8,128)(2,1)S(1)}, u32[]{:S(2)}, u32[]{:S(2)}) async-start(bf16[16,48,128]{2,1,0:T(8,128)(2,1)} %mix.1), calls=%async_computation.1 | async-start | bytes 393216 | tf_op jit(solution)/shard_map/all_to_all | solution.py:398
